TPU v7x, 32 devices: a whole 2x2x4 slice. The times are simulated.
32 devices in a mesh: rep: 2 (over y), fs: 4 (over z), tp: 4 (over x, core).
Axes of the slice: x: 2, y: 2, z: 4, core: 2. Of those that a mesh axis runs over, the one named last changes fastest.
Arguments:
- out_grad: bfloat16 [2048, 2048], P(('rep', 'fs'), 'tp'), may hold values from -6 to 6
- gate_lin: bfloat16 [2048, 5632], P(('rep', 'fs'), 'tp'), may hold values from -6 to 6
- up_lin: bfloat16 [2048, 5632], P(('rep', 'fs'), 'tp'), may hold values from -6 to 6
- conv_weight: bfloat16 [3, 5632], replicated, may hold values from -3.5 to 3.5
- gate_weight: bfloat16 [2048, 5632], P('fs', 'tp'), may hold values from -0.125 to 0.125
- up_weight: bfloat16 [2048, 5632], P('fs', 'tp'), may hold values from -0.125 to 0.125
- down_weight: bfloat16 [5632, 2048], P('tp', 'fs'), may hold values from -0.078125 to 0.078125
Outputs:
- input_grad: bfloat16 [2048, 2048], P(('rep', 'fs'), 'tp')
- conv_grad: float32 [3, 5632], replicated
All inputs are finite; a program needn't handle non-finite values.
Results may differ from a plain program's by a relative error of at most 0.015.
Values may be sent and summed in bfloat16 or wider, within the bound.
A program may use at most 64 MiB of HBM per device.

v0:
```python
import math
import jax
import jax.numpy as jnp
from jax import lax
from jax.sharding import PartitionSpec as P


def extended(value, sides, width):
    for axis, dim in sides:
        peers, length = (lax.axis_size(axis), value.shape[dim])
        up = [(i, (i + 1) % peers) for i in range(peers - 1)]
        down = [(j, i) for i, j in up]
        last = lax.slice_in_dim(value, length - width, length, axis=dim)
        leading = lax.slice_in_dim(value, 0, width, axis=dim)
        before = lax.ppermute(last, axis, up)
        after = lax.ppermute(leading, axis, down)
        value = jnp.concatenate([before, value, after], axis=dim)
    return value


def gelu_parts(gate):
    normal_cdf = 0.5 * (1.0 + jax.scipy.special.erf(gate * (1.0 / math.sqrt(2.0))))
    density = jnp.exp(-0.5 * gate * gate) * (1.0 / math.sqrt(2.0 * math.pi))
    return (gate * normal_cdf, normal_cdf + gate * density)


def local(out_grad, gate_lin, up_lin, conv_weight, gate_weight, up_weight, down_weight):
    conv_full = conv_weight.astype(jnp.float32)
    column_count = gate_lin.shape[1]
    column_start = lax.axis_index("tp") * column_count
    conv_taps = lax.dynamic_slice_in_dim(conv_full, column_start, column_count, 1)
    grad_rows = lax.all_gather(out_grad, "tp", axis=1, tiled=True)
    act_grad = lax.dot_general(
        grad_rows,
        lax.all_gather(down_weight, "fs", axis=1, tiled=True),
        (((1,), (1,)), ((), ())),
        preferred_element_type=jnp.float32,
    )
    linear_mid = extended(gate_lin, (("fs", 0),), 1).astype(jnp.float32)
    gate = (
        conv_taps[0] * linear_mid[:-2]
        + conv_taps[1] * linear_mid[1:-1]
        + conv_taps[2] * linear_mid[2:]
    )
    gelu_value, gelu_slope = gelu_parts(gate)
    gate_grad = act_grad * up_lin.astype(jnp.float32) * gelu_slope
    grad_ext = extended(gate_grad.astype(jnp.bfloat16), (("fs", 0),), 1).astype(gate_grad.dtype)
    up_grad = (act_grad * gelu_value).astype(jnp.bfloat16)
    own_grad = grad_ext[1:-1]
    linear_grad = (
        conv_taps[0] * grad_ext[2:] + conv_taps[1] * own_grad + conv_taps[2] * grad_ext[:-2]
    ).astype(jnp.bfloat16)
    local_conv = jnp.stack(
        [
            jnp.sum(own_grad * linear_mid[:-2], axis=0),
            jnp.sum(own_grad * linear_mid[1:-1], axis=0),
            jnp.sum(own_grad * linear_mid[2:], axis=0),
        ]
    )
    product = lax.dot_general(
        linear_grad,
        lax.all_gather(gate_weight, "fs", axis=0, tiled=True),
        (((1,), (1,)), ((), ())),
        preferred_element_type=jnp.float32,
    )
    product = product + lax.dot_general(
        up_grad,
        lax.all_gather(up_weight, "fs", axis=0, tiled=True),
        (((1,), (1,)), ((), ())),
        preferred_element_type=jnp.float32,
    )
    input_grad = lax.psum_scatter(
        product.astype(jnp.bfloat16), "tp", scatter_dimension=1, tiled=True
    )
    summed_conv = lax.psum(local_conv, ("rep", "fs"))
    conv_grad = lax.all_gather(summed_conv, "tp", axis=1, tiled=True)
    return (input_grad, conv_grad)


def solution(mesh):
    return jax.shard_map(
        local,
        mesh=mesh,
        in_specs=(
            P(("rep", "fs"), "tp"),
            P(("rep", "fs"), "tp"),
            P(("rep", "fs"), "tp"),
            P(),
            P("fs", "tp"),
            P("fs", "tp"),
            P("tp", "fs"),
        ),
        out_specs=(P(("rep", "fs"), "tp"), P()),
        check_vma=False,
    )
```

profile of v0, /device:TPU:0, one launch (start us, length us, event | category | flops | bytes accessed | tf_op | source)
XLA Modules:
  0.0 404.9 jit_solution(1864692760127615159)
XLA Ops:
  7.2 0.7 all-gather.5.cloned.1.call-update
  7.9 0.7 all-gather.7.cloned.1.call-update
  8.7 0.7 all-gather.9.cloned.1.call-update
  9.4 0.5 all-gather.11.cloned.1.call-update
  10.1 5.1 %collective-permute-start = (bf16[1,1408]{1,0:T(2,128)(2,1)S(1)}, bf16[1,1408]{1,0:T(2,128)(2,1)S(1)}, u32[]{:S(2)}, u32[]{:S(2)}) collective-permute-start(bf16[1,1408]{1,0:T(2,128)(2,1)S(1)} %get-tuple-element.12), channel_id=1, source_target_pairs={{0,4},{4,8},{8,12},{1,5},{5,9},{9,13},{2,6},{6,10},{10,14},{3,7},{... | collective-permute-start | bytes 8456 | tf_op jit(solution)/shard_map/ppermute | solution.py:15
  15.2 1.3 collective-permute-start.1
  16.5 0.7 dynamic-slice_convert_fusion
  17.2 3.4 collective-permute-done.1
  20.7 0.2 maximum_convert_fusion
  20.8 8.2 %all-gather.5.cloned.1.call-done = bf16[256,2048]{1,0:T(8,128)(2,1)} async-done(((bf16[256,512]{1,0:T(8,128)(2,1)}), bf16[256,2048]{1,0:T(8,128)(2,1)}) %all-gather.5.cloned.1.call-update) | async-done | bytes 1048592 | tf_op jit(solution)/shard_map/all_gather | solution.py:32
  29.0 108.3 %all-gather.7.cloned.1.call-done = bf16[1408,2048]{1,0:T(8,128)(2,1)} async-done(((bf16[1408,512]{1,0:T(8,128)(2,1)}), bf16[1408,2048]{1,0:T(8,128)(2,1)}) %all-gather.7.cloned.1.call-update) | async-done | bytes 5767184 | tf_op jit(solution)/shard_map/all_gather | solution.py:35
  137.3 7.2 %fusion.6 = (bf16[256,1408]{1,0:T(8,128)(2,1)S(1)}, f32[256,1408]{1,0:T(8,128)}, f32[256,1408]{1,0:T(8,128)}) fusion(bf16[256,1408]{1,0:T(8,128)(2,1)S(1)} %copy-done.1, f32[258,1408]{1,0:T(8,128)S(1)} %maximum_convert_fusion, f32[1408]{0:T(1024)S(1)} %get-tuple-element.7, f32[1408]{0:T(1024)S(1)} %get-tuple-element.6, f32[1408]{0:T(1024)S(1)} %get-tuple-element.5, ...), kind=kOutput, calls=%fused_computation.8 | convolution fusion | flops 1482522624 | bytes 15483392 | tf_op jit(solution)/shard_map/dot_general | solution.py:33
  144.5 1.3 collective-permute-start.2
  145.8 1.3 collective-permute-start.3
  147.1 4.4 %collective-permute-done.3 = bf16[1,1408]{1,0:T(2,128)(2,1)S(1)} collective-permute-done((bf16[1,1408]{1,0:T(2,128)(2,1)S(1)}, bf16[1,1408]{1,0:T(2,128)(2,1)S(1)}, u32[]{:S(2)}, u32[]{:S(2)}) %collective-permute-start.3) | collective-permute-done | bytes 2848 | tf_op jit(solution)/shard_map/ppermute | solution.py:16
  151.5 0.2 maximum_convert_fusion.1
  151.7 92.3 %all-gather.9.cloned.1.call-done = bf16[2048,1408]{1,0:T(8,128)(2,1)} async-done(((bf16[512,1408]{1,0:T(8,128)(2,1)}), bf16[2048,1408]{1,0:T(8,128)(2,1)}) %all-gather.9.cloned.1.call-update) | async-done | bytes 5767184 | tf_op jit(solution)/shard_map/all_gather | solution.py:62
  244.0 6.0 %fusion.10 = f32[256,2048]{1,0:T(8,128)} fusion(bf16[2048,1408]{1,0:T(8,128)(2,1)} %all-gather.9.cloned.1.call-done, f32[258,1408]{1,0:T(8,128)S(1)} %maximum_convert_fusion.1, f32[1408]{0:T(1024)S(1)} %get-tuple-element.7, f32[1408]{0:T(1024)S(1)} %get-tuple-element.6, f32[1408]{0:T(1024)S(1)} %get-tuple-element.5), kind=kOutput, calls=%fused_computation.22 | convolution fusion | flops 1478557696 | bytes 12214272 | tf_op jit(solution)/shard_map/dot_general | solution.py:60
  249.9 100.4 %all-gather.11.cloned.1.call-done = bf16[2048,1408]{1,0:T(8,128)(2,1)} async-done(((bf16[512,1408]{1,0:T(8,128)(2,1)}), bf16[2048,1408]{1,0:T(8,128)(2,1)}) %all-gather.11.cloned.1.call-update) | async-done | bytes 5767184 | tf_op jit(solution)/shard_map/all_gather | solution.py:68
  350.3 6.9 %fusion = bf16[256,2048]{1,0:T(8,128)(2,1)} fusion(f32[256,2048]{1,0:T(8,128)} %fusion.10, bf16[2048,1408]{1,0:T(8,128)(2,1)} %all-gather.11.cloned.1.call-done, f32[256,1408]{1,0:T(8,128)} %get-tuple-element.14, f32[256,1408]{1,0:T(8,128)} %get-tuple-element.9), kind=kOutput, calls=%fused_computation.1 | convolution fusion | flops 1479606272 | bytes 11796480 | tf_op jit(solution)/shard_map/dot_general | solution.py:66
  357.3 0.6 multiply_reduce_fusion.2
  357.9 34.5 %psum.7 = f32[3,1408]{1,0:T(4,128)S(1)} all-reduce(f32[3,1408]{1,0:T(4,128)S(1)} %pad_maximum_fusion), channel_id=1, replica_groups=mesh['rep'=2,'fs'=4,'tp'=4] {'rep','fs'}, use_global_device_ids=true, to_apply=%region_4.0 | all-reduce | flops 4224 | bytes 33792 | tf_op jit(solution)/shard_map/psum | solution.py:75
  392.4 5.3 %all_gather.19 = f32[3,5632]{1,0:T(4,128)S(1)} all-gather(f32[3,1408]{1,0:T(4,128)S(1)} %psum.7), channel_id=1, replica_groups=mesh['rep'=2,'fs'=4,'tp'=4] {'tp'}, dimensions={1}, use_global_device_ids=true | all-gather | bytes 84480 | tf_op jit(solution)/shard_map/all_gather | solution.py:76
  397.7 0.6 copy.10
  (20 shorter events, 0.4 us)
Async XLA Ops:
  7.2 21.8 %all-gather.5.cloned.1.call-start = ((), (), s32[]{:S(2)}) async-start(), calls=%async_computation.1 | async-start | bytes 1310720 | tf_op jit(solution)/shard_map/all_gather | solution.py:32
  7.9 129.4 %all-gather.7.cloned.1.call-start = ((), (), s32[]{:S(2)}) async-start(), calls=%async_computation.2 | async-start | bytes 7208960 | tf_op jit(solution)/shard_map/all_gather | solution.py:35
  8.6 1.4 copy-start
  8.7 235.3 %all-gather.9.cloned.1.call-start = ((), (), s32[]{:S(2)}) async-start(), calls=%async_computation.3 | async-start | bytes 7208960 | tf_op jit(solution)/shard_map/all_gather | solution.py:62
  9.4 340.9 %all-gather.11.cloned.1.call-start = ((), (), s32[]{:S(2)}) async-start(), calls=%async_computation.4 | async-start | bytes 7208960 | tf_op jit(solution)/shard_map/all_gather | solution.py:68
  10.0 127.3 %copy-start.1 = (bf16[256,1408]{1,0:T(8,128)(2,1)S(1)}, bf16[256,1408]{1,0:T(8,128)(2,1)}, u32[]{:S(2)}) copy-start(bf16[256,1408]{1,0:T(8,128)(2,1)} %param.9) | copy-start | bytes 2162692
  10.0 387.7 %reduce-scatter.2.cloned.1.call-start = ((), (), s32[]{:S(2)}) async-start(), calls=%async_computation.5 | async-start | bytes 1310720 | tf_op jit(solution)/shard_map/reduce_scatter | solution.py:72
  10.1 7.2 %collective-permute-start = (bf16[1,1408]{1,0:T(2,128)(2,1)S(1)}, bf16[1,1408]{1,0:T(2,128)(2,1)S(1)}, u32[]{:S(2)}, u32[]{:S(2)}) collective-permute-start(bf16[1,1408]{1,0:T(2,128)(2,1)S(1)} %get-tuple-element.12), channel_id=1, source_target_pairs={{0,4},{4,8},{8,12},{1,5},{5,9},{9,13},{2,6},{6,10},{10,14},{3,7},{... | collective-permute-start | bytes 8456 | tf_op jit(solution)/shard_map/ppermute | solution.py:15
  15.2 5.5 %collective-permute-start.1 = (bf16[1,1408]{1,0:T(2,128)(2,1)S(1)}, bf16[1,1408]{1,0:T(2,128)(2,1)S(1)}, u32[]{:S(2)}, u32[]{:S(2)}) collective-permute-start(bf16[1,1408]{1,0:T(2,128)(2,1)S(1)} %get-tuple-element.13), channel_id=1, source_target_pairs={{4,0},{8,4},{12,8},{5,1},{9,5},{13,9},{6,2},{10,6},{14,10},{7,3},{... | collective-permute-start | bytes 8456 | tf_op jit(solution)/shard_map/ppermute | solution.py:16
  144.5 2.6 collective-permute-start.2
  145.8 5.8 %collective-permute-start.3 = (bf16[1,1408]{1,0:T(2,128)(2,1)S(1)}, bf16[1,1408]{1,0:T(2,128)(2,1)S(1)}, u32[]{:S(2)}, u32[]{:S(2)}) collective-permute-start(bf16[1,1408]{1,0:T(2,128)(2,1)S(1)} %get-tuple-element.11), channel_id=1, source_target_pairs={{4,0},{8,4},{12,8},{5,1},{9,5},{13,9},{6,2},{10,6},{14,10},{7,3},{... | collective-permute-start | bytes 8456 | tf_op jit(solution)/shard_map/ppermute | solution.py:16
Sparse Core Ops, SparseCore 0:
  9.5 19.4 all-gather.4
  30.6 106.6 all-gather.6
  138.9 105.0 all-gather.8
  245.4 104.8 all-gather.10
  357.4 23.0 reduce-scatter.1
where the time goes:
time: 405 us
  waiting for transfers between devices  320 us (79%)
  blocking collectives  39.8 us (10%)
  matrix products  20.1 us (5%)
  between operations  13.9 us (3%)
  starting transfers between devices  9.15 us (2%)
    all_gather x1, waiting for transfers between devices, local(): lax.all_gather(down_weight, 'fs', axis=1, tiled=True)  108 us
    all_gather x1, waiting for transfers between devices, local(): lax.all_gather(up_weight, 'fs', axis=0, tiled=True)  100 us
    all_gather x1, waiting for transfers between devices, local(): lax.all_gather(gate_weight, 'fs', axis=0, tiled=True)  92.3 us
    psum x1, blocking collectives, local(): summed_conv = lax.psum(local_conv, ('rep', 'fs'))  34.5 us
    all_gather x1, waiting for transfers between devices, local(): grad_rows = lax.all_gather(out_grad, 'tp', axis=1, tiled=True)  8.16 us
  transfers between devices with their start and end apart: 9, of which 6 were waited for; matrix products, arithmetic and copies ran while one was open for 4% of the time, Pallas kernels for 0%

commit v1 on v0

--- a/solution.py
+++ b/solution.py
@@ -72,7 +72,7 @@
     input_grad = lax.psum_scatter(
         product.astype(jnp.bfloat16), "tp", scatter_dimension=1, tiled=True
     )
-    summed_conv = lax.psum(local_conv, ("rep", "fs"))
+    summed_conv = lax.psum(lax.psum(local_conv, "fs"), "rep")
     conv_grad = lax.all_gather(summed_conv, "tp", axis=1, tiled=True)
     return (input_grad, conv_grad)
 

time: 405 us -> 395 us (0.975)
  blocking collectives: 39.8 us -> 29.7 us
    psum x1 -> x2, blocking collectives: 34.5 us -> 24.4 us  [local(): summed_conv = lax.psum(lax.psum(local_conv, 'fs'), 'rep')]
where the time goes in v1:
time: 395 us
  waiting for transfers between devices  320 us (81%)
  blocking collectives  29.7 us (8%)
  matrix products  20 us (5%)
  between operations  13.9 us (4%)
  starting transfers between devices  9.15 us (2%)
    all_gather x1, waiting for transfers between devices, local(): lax.all_gather(down_weight, 'fs', axis=1, tiled=True)  108 us
    all_gather x1, waiting for transfers between devices, local(): lax.all_gather(up_weight, 'fs', axis=0, tiled=True)  100 us
    all_gather x1, waiting for transfers between devices, local(): lax.all_gather(gate_weight, 'fs', axis=0, tiled=True)  92.3 us
    psum x2, blocking collectives, local(): summed_conv = lax.psum(lax.psum(local_conv, 'fs'), 'rep')  24.4 us
    all_gather x1, waiting for transfers between devices, local(): grad_rows = lax.all_gather(out_grad, 'tp', axis=1, tiled=True)  8.16 us
  transfers between devices with their start and end apart: 9, of which 6 were waited for; matrix products, arithmetic and copies ran while one was open for 4% of the time, Pallas kernels for 0%

profile of v1, /device:TPU:0, one launch (start us, length us, event | category | flops | bytes accessed | tf_op | source)
XLA Modules:
  0.0 394.8 jit_solution(10878238102943732399)
XLA Ops:
  7.2 0.7 all-gather.5.cloned.1.call-update
  7.9 0.7 all-gather.7.cloned.1.call-update
  8.7 0.7 all-gather.9.cloned.1.call-update
  9.4 0.5 all-gather.11.cloned.1.call-update
  10.1 5.1 %collective-permute-start = (bf16[1,1408]{1,0:T(2,128)(2,1)S(1)}, bf16[1,1408]{1,0:T(2,128)(2,1)S(1)}, u32[]{:S(2)}, u32[]{:S(2)}) collective-permute-start(bf16[1,1408]{1,0:T(2,128)(2,1)S(1)} %get-tuple-element.12), channel_id=1, source_target_pairs={{0,4},{4,8},{8,12},{1,5},{5,9},{9,13},{2,6},{6,10},{10,14},{3,7},{... | collective-permute-start | bytes 8456 | tf_op jit(solution)/shard_map/ppermute | solution.py:15
  15.2 1.3 collective-permute-start.1
  16.5 0.7 dynamic-slice_convert_fusion
  17.2 3.4 collective-permute-done.1
  20.8 8.2 %all-gather.5.cloned.1.call-done = bf16[256,2048]{1,0:T(8,128)(2,1)} async-done(((bf16[256,512]{1,0:T(8,128)(2,1)}), bf16[256,2048]{1,0:T(8,128)(2,1)}) %all-gather.5.cloned.1.call-update) | async-done | bytes 1048592 | tf_op jit(solution)/shard_map/all_gather | solution.py:32
  29.0 108.3 %all-gather.7.cloned.1.call-done = bf16[1408,2048]{1,0:T(8,128)(2,1)} async-done(((bf16[1408,512]{1,0:T(8,128)(2,1)}), bf16[1408,2048]{1,0:T(8,128)(2,1)}) %all-gather.7.cloned.1.call-update) | async-done | bytes 5767184 | tf_op jit(solution)/shard_map/all_gather | solution.py:35
  137.3 7.2 %fusion.6 = (bf16[256,1408]{1,0:T(8,128)(2,1)S(1)}, f32[256,1408]{1,0:T(8,128)}, f32[256,1408]{1,0:T(8,128)}) fusion(bf16[256,1408]{1,0:T(8,128)(2,1)S(1)} %copy-done.1, f32[258,1408]{1,0:T(8,128)S(1)} %maximum_convert_fusion, f32[1408]{0:T(1024)S(1)} %get-tuple-element.7, f32[1408]{0:T(1024)S(1)} %get-tuple-element.6, f32[1408]{0:T(1024)S(1)} %get-tuple-element.5, ...), kind=kOutput, calls=%fused_computation.8 | convolution fusion | flops 1482522624 | bytes 15483392 | tf_op jit(solution)/shard_map/dot_general | solution.py:33
  144.5 1.3 collective-permute-start.2
  145.8 1.3 collective-permute-start.3
  147.1 4.4 %collective-permute-done.3 = bf16[1,1408]{1,0:T(2,128)(2,1)S(1)} collective-permute-done((bf16[1,1408]{1,0:T(2,128)(2,1)S(1)}, bf16[1,1408]{1,0:T(2,128)(2,1)S(1)}, u32[]{:S(2)}, u32[]{:S(2)}) %collective-permute-start.3) | collective-permute-done | bytes 2848 | tf_op jit(solution)/shard_map/ppermute | solution.py:16
  151.5 0.2 maximum_convert_fusion.1
  151.7 92.3 %all-gather.9.cloned.1.call-done = bf16[2048,1408]{1,0:T(8,128)(2,1)} async-done(((bf16[512,1408]{1,0:T(8,128)(2,1)}), bf16[2048,1408]{1,0:T(8,128)(2,1)}) %all-gather.9.cloned.1.call-update) | async-done | bytes 5767184 | tf_op jit(solution)/shard_map/all_gather | solution.py:62
  244.0 6.0 %fusion.10 = f32[256,2048]{1,0:T(8,128)} fusion(bf16[2048,1408]{1,0:T(8,128)(2,1)} %all-gather.9.cloned.1.call-done, f32[258,1408]{1,0:T(8,128)S(1)} %maximum_convert_fusion.1, f32[1408]{0:T(1024)S(1)} %get-tuple-element.7, f32[1408]{0:T(1024)S(1)} %get-tuple-element.6, f32[1408]{0:T(1024)S(1)} %get-tuple-element.5), kind=kOutput, calls=%fused_computation.22 | convolution fusion | flops 1478557696 | bytes 12214272 | tf_op jit(solution)/shard_map/dot_general | solution.py:60
  249.9 100.4 %all-gather.11.cloned.1.call-done = bf16[2048,1408]{1,0:T(8,128)(2,1)} async-done(((bf16[512,1408]{1,0:T(8,128)(2,1)}), bf16[2048,1408]{1,0:T(8,128)(2,1)}) %all-gather.11.cloned.1.call-update) | async-done | bytes 5767184 | tf_op jit(solution)/shard_map/all_gather | solution.py:68
  350.3 6.9 %fusion = bf16[256,2048]{1,0:T(8,128)(2,1)} fusion(f32[256,2048]{1,0:T(8,128)} %fusion.10, bf16[2048,1408]{1,0:T(8,128)(2,1)} %all-gather.11.cloned.1.call-done, f32[256,1408]{1,0:T(8,128)} %get-tuple-element.14, f32[256,1408]{1,0:T(8,128)} %get-tuple-element.9), kind=kOutput, calls=%fused_computation.1 | convolution fusion | flops 1479606272 | bytes 11796480 | tf_op jit(solution)/shard_map/dot_general | solution.py:66
  357.3 0.6 multiply_reduce_fusion.2
  357.9 16.0 %psum.14 = f32[3,1408]{1,0:T(4,128)S(1)} all-reduce(f32[3,1408]{1,0:T(4,128)S(1)} %pad_maximum_fusion), channel_id=1, replica_groups=mesh['rep'=2,'fs'=4,'tp'=4] {'fs'}, use_global_device_ids=true, to_apply=%region_4.0 | all-reduce | flops 4224 | bytes 33792 | tf_op jit(solution)/shard_map/psum | solution.py:75
  374.0 8.4 %psum.15 = f32[3,1408]{1,0:T(4,128)S(1)} all-reduce(f32[3,1408]{1,0:T(4,128)S(1)} %psum.14), channel_id=1, replica_groups=mesh['rep'=2,'fs'=4,'tp'=4] {'rep'}, use_global_device_ids=true, to_apply=%region_5.0 | all-reduce | flops 4224 | bytes 33792 | tf_op jit(solution)/shard_map/psum | solution.py:75
  382.4 5.3 %all_gather.19 = f32[3,5632]{1,0:T(4,128)S(1)} all-gather(f32[3,1408]{1,0:T(4,128)S(1)} %psum.15), channel_id=1, replica_groups=mesh['rep'=2,'fs'=4,'tp'=4] {'tp'}, dimensions={1}, use_global_device_ids=true | all-gather | bytes 84480 | tf_op jit(solution)/shard_map/all_gather | solution.py:76
  387.7 0.6 copy.10
  (21 shorter events, 0.5 us)
Async XLA Ops:
  7.2 21.8 %all-gather.5.cloned.1.call-start = ((), (), s32[]{:S(2)}) async-start(), calls=%async_computation.1 | async-start | bytes 1310720 | tf_op jit(solution)/shard_map/all_gather | solution.py:32
  7.9 129.4 %all-gather.7.cloned.1.call-start = ((), (), s32[]{:S(2)}) async-start(), calls=%async_computation.2 | async-start | bytes 7208960 | tf_op jit(solution)/shard_map/all_gather | solution.py:35
  8.6 1.4 copy-start
  8.7 235.3 %all-gather.9.cloned.1.call-start = ((), (), s32[]{:S(2)}) async-start(), calls=%async_computation.3 | async-start | bytes 7208960 | tf_op jit(solution)/shard_map/all_gather | solution.py:62
  9.4 340.9 %all-gather.11.cloned.1.call-start = ((), (), s32[]{:S(2)}) async-start(), calls=%async_computation.4 | async-start | bytes 7208960 | tf_op jit(solution)/shard_map/all_gather | solution.py:68
  10.0 127.3 %copy-start.1 = (bf16[256,1408]{1,0:T(8,128)(2,1)S(1)}, bf16[256,1408]{1,0:T(8,128)(2,1)}, u32[]{:S(2)}) copy-start(bf16[256,1408]{1,0:T(8,128)(2,1)} %param.9) | copy-start | bytes 2162692
  10.0 377.7 %reduce-scatter.2.cloned.1.call-start = ((), (), s32[]{:S(2)}) async-start(), calls=%async_computation.5 | async-start | bytes 1310720 | tf_op jit(solution)/shard_map/reduce_scatter | solution.py:72
  10.1 7.2 %collective-permute-start = (bf16[1,1408]{1,0:T(2,128)(2,1)S(1)}, bf16[1,1408]{1,0:T(2,128)(2,1)S(1)}, u32[]{:S(2)}, u32[]{:S(2)}) collective-permute-start(bf16[1,1408]{1,0:T(2,128)(2,1)S(1)} %get-tuple-element.12), channel_id=1, source_target_pairs={{0,4},{4,8},{8,12},{1,5},{5,9},{9,13},{2,6},{6,10},{10,14},{3,7},{... | collective-permute-start | bytes 8456 | tf_op jit(solution)/shard_map/ppermute | solution.py:15
  15.2 5.5 %collective-permute-start.1 = (bf16[1,1408]{1,0:T(2,128)(2,1)S(1)}, bf16[1,1408]{1,0:T(2,128)(2,1)S(1)}, u32[]{:S(2)}, u32[]{:S(2)}) collective-permute-start(bf16[1,1408]{1,0:T(2,128)(2,1)S(1)} %get-tuple-element.13), channel_id=1, source_target_pairs={{4,0},{8,4},{12,8},{5,1},{9,5},{13,9},{6,2},{10,6},{14,10},{7,3},{... | collective-permute-start | bytes 8456 | tf_op jit(solution)/shard_map/ppermute | solution.py:16
  144.5 2.6 collective-permute-start.2
  145.8 5.8 %collective-permute-start.3 = (bf16[1,1408]{1,0:T(2,128)(2,1)S(1)}, bf16[1,1408]{1,0:T(2,128)(2,1)S(1)}, u32[]{:S(2)}, u32[]{:S(2)}) collective-permute-start(bf16[1,1408]{1,0:T(2,128)(2,1)S(1)} %get-tuple-element.11), channel_id=1, source_target_pairs={{4,0},{8,4},{12,8},{5,1},{9,5},{13,9},{6,2},{10,6},{14,10},{7,3},{... | collective-permute-start | bytes 8456 | tf_op jit(solution)/shard_map/ppermute | solution.py:16
Sparse Core Ops, SparseCore 0:
  9.5 19.4 all-gather.4
  30.6 106.6 all-gather.6
  138.9 105.0 all-gather.8
  245.4 104.8 all-gather.10
  357.4 23.0 reduce-scatter.1
